TPU v7x, 32 devices: a whole 2x2x4 slice. The times are simulated.
32 devices in a mesh: dp: 4 (over y, x), kv: 4 (over z), tp: 2 (over core).
Axes of the slice: x: 2, y: 2, z: 4, core: 2. Of those that a mesh axis runs over, the one named last changes fastest.
Arguments:
- tokens: bfloat16 [32, 4096], P('dp', ('kv', 'tp')), as said below
- query_weight: bfloat16 [4096, 16, 128], P(None, 'tp', 'kv'), may hold values from -0.09375 to 0.09375
- key_weight: bfloat16 [4096, 16, 128], P(None, 'tp', 'kv'), may hold values from -0.09375 to 0.09375
- value_weight: bfloat16 [4096, 16, 256], P(None, 'tp', 'kv'), may hold values from -0.09375 to 0.09375
- gate_weight: bfloat16 [4096, 16, 256], P(None, 'tp', 'kv'), may hold values from -0.09375 to 0.09375
- decay_weight: bfloat16 [4096, 16, 128], P(None, 'tp', 'kv'), may hold values from -0.09375 to 0.09375
- decay_bias: float32 [16, 128], P('tp'), may hold values from -8 to 2
- states: float32 [32, 16, 128, 256], P(('dp', 'kv'), 'tp'), may hold values from -4 to 4
- head_gain: float32 [16, 256], P('tp'), may hold values from 0.1 to 1.9
- out_weight: bfloat16 [4096, 4096], P(None, ('kv', 'tp')), as said below
- norm1_gain: float32 [4096], P(('kv', 'tp')), may hold values from 0.1 to 1.9
- norm1_bias: float32 [4096], P(('kv', 'tp')), may hold values from -3 to 3
- up_weight: bfloat16 [4096, 16384], P(None, ('kv', 'tp')), may hold values from -0.09375 to 0.09375
- down_weight: bfloat16 [16384, 4096], P(('kv', 'tp')), as said below
- norm2_gain: float32 [4096], P(('kv', 'tp')), may hold values from 0.1 to 1.9
- norm2_bias: float32 [4096], P(('kv', 'tp')), may hold values from -3 to 3
Outputs:
- layer_out: bfloat16 [32, 4096], P('dp', ('kv', 'tp'))
- new_states: float32 [32, 16, 128, 256], P(('dp', 'kv'), 'tp')
Inputs may be any that keep to these rules, and one draw needn't show every extreme that they name: `tokens`: each block of 64 features has its own scale. `out_weight`: entries lie within 13 / sqrt(4096) of zero. `down_weight`: entries lie within 14 / sqrt(16384) of zero.
All inputs are finite; a program needn't handle non-finite values.
Results may differ from a plain program's by a relative error of at most 0.009.
Values may be sent and summed in bfloat16 or wider, within the bound.
A program may use at most 128 MiB of HBM per device.

v0:
```python
import jax
import jax.numpy as jnp
from jax import lax
from jax.sharding import PartitionSpec as P

D = 4096
KEY_DIM = 128
ALPHA = 2.0**0.5
TAU = 16.0
LN_EPS = 1e-05
RMS_EPS = 1e-06


def project_flat(inputs, weight):
    flattened = weight.reshape(weight.shape[0], -1)
    return jnp.dot(inputs, flattened, preferred_element_type=jnp.float32).astype(jnp.bfloat16)


def normalize(inputs, average, spread, row_gain, row_shift):
    return ((inputs - average) * lax.rsqrt(spread + LN_EPS) * row_gain + row_shift).astype(
        jnp.bfloat16
    )


def body(
    tokens,
    query_weight,
    key_weight,
    value_weight,
    gate_weight,
    decay_weight,
    decay_bias,
    states,
    head_gain,
    out_weight,
    norm1_gain,
    norm1_bias,
    up_weight,
    down_weight,
    norm2_gain,
    norm2_bias,
):
    whole = lax.all_gather(tokens, ("kv", "tp"), axis=1, tiled=True)
    weights_list = (query_weight, key_weight, decay_weight, value_weight, gate_weight)
    packed = jnp.concatenate([project_flat(whole, weight) for weight in weights_list], axis=1)
    arrived = lax.all_to_all(packed, "kv", split_axis=0, concat_axis=0, tiled=True)
    groups = lax.axis_size("kv")
    seq_count = whole.shape[0] // groups
    local_heads = query_weight.shape[1]
    unpacked = []
    start = 0
    for weight in weights_list:
        channels = weight.shape[2]
        width = local_heads * channels
        block = arrived[:, start : start + width].reshape(groups, seq_count, local_heads, channels)
        block = block.transpose(1, 2, 0, 3).reshape(seq_count, local_heads, groups * channels)
        unpacked.append(block.astype(jnp.float32))
        start = start + width
    query_rows = unpacked[0] * KEY_DIM ** (-0.5)
    key_rows = unpacked[1]
    decay_rows = unpacked[2]
    value_rows = unpacked[3]
    gate_rows = unpacked[4]
    retain = jnp.exp(jax.nn.log_sigmoid(decay_rows + decay_bias) / TAU)
    new_states = retain[..., None] * states + key_rows[..., :, None] * value_rows[..., None, :]
    readout = jnp.einsum("shk,shkv->shv", query_rows, new_states, precision=lax.Precision.HIGHEST)
    readout = (
        readout
        * lax.rsqrt(jnp.mean(readout * readout, axis=-1, keepdims=True) + RMS_EPS)
        * head_gain
    )
    attended = (readout * jax.nn.silu(gate_rows)).astype(jnp.bfloat16)
    seq_count, local_heads, value_width = attended.shape
    flat_width = local_heads * value_width
    collected = lax.all_gather(
        attended.reshape(1, seq_count, flat_width), ("kv", "tp"), axis=0, tiled=True
    )
    halves = lax.axis_size("tp")
    collected = collected.reshape(-1, halves, seq_count, flat_width)
    columns = out_weight.shape[1]
    out_parts = out_weight.reshape(halves, flat_width, columns)
    mixed_heads = jnp.einsum(
        "atsc,tcd->asd", collected, out_parts, preferred_element_type=jnp.float32
    ).reshape(-1, columns)
    residual_one = ALPHA * tokens.astype(jnp.float32) + mixed_heads
    offset = lax.axis_index(("kv", "tp")) * columns
    totals = lax.psum(
        (
            jnp.sum(residual_one, axis=-1, keepdims=True),
            jnp.sum(residual_one * residual_one, axis=-1, keepdims=True),
        ),
        ("kv", "tp"),
    )
    average = totals[0] / D
    spread = totals[1] / D - average * average
    normed_own = normalize(residual_one, average, spread, norm1_gain, norm1_bias)
    normed = lax.all_gather(normed_own, ("kv", "tp"), axis=1, tiled=True)
    lifted = jnp.dot(normed, up_weight, preferred_element_type=jnp.float32)
    hidden = jnp.square(jax.nn.relu(lifted)).astype(jnp.bfloat16)
    mixer_term = jnp.dot(hidden, down_weight, preferred_element_type=jnp.float32)
    mixer_all = lax.psum(mixer_term, ("kv", "tp"))
    residual_two = ALPHA * normed.astype(jnp.float32) + mixer_all
    average = jnp.sum(residual_two, axis=-1, keepdims=True) / D
    spread = jnp.sum(residual_two * residual_two, axis=-1, keepdims=True) / D - average * average
    own_rows = lax.dynamic_slice_in_dim(residual_two, offset, columns, 1)
    layer_out = normalize(own_rows, average, spread, norm2_gain, norm2_bias)
    return (layer_out, new_states)


def solution(mesh):
    placed = (
        P("dp", ("kv", "tp")),
        P(None, "tp", "kv"),
        P(None, "tp", "kv"),
        P(None, "tp", "kv"),
        P(None, "tp", "kv"),
        P(None, "tp", "kv"),
        P("tp", None),
        P(("dp", "kv"), "tp", None, None),
        P("tp", None),
        P(None, ("kv", "tp")),
        P(("kv", "tp")),
        P(("kv", "tp")),
        P(None, ("kv", "tp")),
        P(("kv", "tp"), None),
        P(("kv", "tp")),
        P(("kv", "tp")),
    )
    return jax.shard_map(
        body,
        mesh=mesh,
        in_specs=placed,
        out_specs=(P("dp", ("kv", "tp")), P(("dp", "kv"), "tp", None, None)),
        check_vma=False,
    )
```

profile of v0, /device:TPU:0, one launch (start us, length us, event | category | flops | bytes accessed | tf_op | source)
XLA Modules:
  0.0 167.2 jit_solution(12161936013294554536)
XLA Ops:
  7.2 0.0 copy-start
  7.2 0.0 all-reduce.3.cloned.1.call-start
  7.2 0.0 copy-start.4
  7.2 16.0 %all_gather.9 = bf16[8,4096]{1,0:T(8,128)(2,1)S(1)} all-gather(bf16[8,512]{1,0:T(8,128)(2,1)} %param.16), channel_id=1, replica_groups=mesh['dp'=4,'kv'=4,'tp'=2] {'kv','tp'}, dimensions={1}, use_global_device_ids=true | all-gather | bytes 73728 | tf_op jit(solution)/shard_map/all_gather | solution.py:43
  23.3 0.0 copy-done
  23.3 0.6 fusion.7
  23.9 0.0 copy-done.4
  23.9 0.7 fusion.6
  24.6 2.6 %fusion.5 = bf16[8,1792]{1,0:T(8,128)(2,1)S(1)} fusion(bf16[8,1792]{1,0:T(8,128)(2,1)S(1)} %fusion.6, bf16[8,4096]{1,0:T(8,128)(2,1)S(1)} %all_gather.9, bf16[4096,256]{0,1:T(8,128)(2,1)} %bitcast.60), kind=kOutput, calls=%fused_computation.11 | convolution fusion | flops 16779264 | bytes 2166784 | tf_op jit(solution)/shard_map/dot_general | solution.py:16
  27.2 0.0 copy-done.2
  27.2 1.2 fusion.4
  28.4 1.0 copy-done.3
  29.4 1.2 fusion.3
  30.6 10.1 %all_to_all.12 = bf16[4,2,1792]{2,1,0:T(2,128)(2,1)S(1)} all-to-all(bf16[4,2,1792]{2,1,0:T(2,128)(2,1)S(1)} %all_to_all.8), channel_id=1, replica_groups=mesh['dp'=4,'kv'=4,'tp'=2] {'kv'}, dimensions={0} | all-to-all | bytes 57344 | tf_op jit(solution)/shard_map/all_to_all | solution.py:46
  40.7 0.1 reshape.138
  40.8 0.1 reshape.134
  40.9 0.1 reshape.136
  41.0 0.1 reshape.132
  41.1 0.1 reshape.137
  41.2 0.1 reshape.133
  41.3 0.1 mul.135
  41.4 0.1 reshape.140
  41.4 0.0 copy-done.7
  41.5 1.9 %multiply_add_fusion = f32[2,8,128,256]{3,2,1,0:T(8,128)S(1)} fusion(f32[2,8,128,256]{3,2,1,0:T(8,128)} %param.23, f32[2,8,256]{2,1,0:T(8,128)S(1)} %reshape.134, f32[2,8,128]{2,1,0:T(8,128)S(1)} %reshape.133, f32[2,8,128]{2,1,0:T(8,128)S(1)} %fusion.16), kind=kLoop, calls=%fused_computation.3 | loop fusion | flops 1572864 | bytes 4227072 | tf_op jit(solution)/shard_map/add | solution.py:65
  43.4 0.0 copy-start.1
  43.4 0.0 copy-start.6
  43.4 0.0 copy-start.5
  43.4 1.3 copy-done.1
  44.7 1.1 fusion.20
  45.8 0.1 fusion.10
  45.9 0.1 reshape.139
  46.0 0.1 reshape.135
  46.1 0.0 copy-done.6
  46.1 0.1 fusion.13
  46.2 14.0 %all_gather.10 = bf16[8,2,2048]{2,1,0:T(2,128)(2,1)S(1)} all-gather(bf16[1,2,2048]{2,1,0:T(2,128)(2,1)S(1)} %reshape.129), channel_id=1, replica_groups=mesh['dp'=4,'kv'=4,'tp'=2] {'kv','tp'}, dimensions={0}, use_global_device_ids=true | all-gather | bytes 73728 | tf_op jit(solution)/shard_map/all_gather | solution.py:75
  60.3 0.0 copy-done.5
  60.3 0.0 copy-start.8
  60.3 0.0 copy-start.9
  60.3 3.0 %fusion.19 = (f32[8]{0:T(128)S(1)}, f32[8]{0:T(128)S(1)}, f32[8,512]{1,0:T(8,128)S(1)}) fusion(bf16[8,2048,2]{1,0,2:T(8,128)(2,1)S(1)} %dot_general.38, bf16[2,2048,512]{2,1,0:T(8,128)(2,1)} %bitcast.56, bf16[8,512]{1,0:T(8,128)(2,1)S(1)} %copy-done.5), kind=kOutput, calls=%fused_computation.45 | convolution fusion | flops 33578992 | bytes 4284480 | tf_op jit(solution)/shard_map/atsc,tcd->asd/dot_general | solution.py:82
  63.3 14.2 %all-reduce = (f32[8,1]{0,1:T(1,128)S(1)}, f32[8,1]{0,1:T(1,128)S(1)}) all-reduce(f32[8,1]{0,1:T(1,128)S(1)} %bitcast.69, f32[8,1]{0,1:T(1,128)S(1)} %bitcast.68), channel_id=1, replica_groups=mesh['dp'=4,'kv'=4,'tp'=2] {'kv','tp'}, use_global_device_ids=true, to_apply=%region_4.5 | all-reduce | flops 16 | bytes 128 | tf_op jit(solution)/shard_map/psum | solution.py:87
  77.6 0.0 copy-done.9
  77.6 0.1 add_convert_fusion.1
  77.7 14.0 %all_gather.11 = bf16[8,4096]{1,0:T(8,128)(2,1)S(1)} all-gather(bf16[8,512]{1,0:T(8,128)(2,1)S(1)} %add_convert_fusion.1), channel_id=1, replica_groups=mesh['dp'=4,'kv'=4,'tp'=2] {'kv','tp'}, dimensions={1}, use_global_device_ids=true | all-gather | bytes 73728 | tf_op jit(solution)/shard_map/all_gather | solution.py:97
  91.6 13.5 %fusion.8 = f32[8,4096]{1,0:T(8,128)} fusion(bf16[2048,4096]{1,0:T(8,128)(2,1)} %param.29, bf16[8,4096]{1,0:T(8,128)(2,1)S(1)} %all_gather.11, bf16[4096,2048]{1,0:T(8,128)(2,1)} %param.28), kind=kOutput, calls=%fused_computation.16 | convolution fusion | flops 268484608 | bytes 33751040 | tf_op jit(solution)/shard_map/dot_general | solution.py:100
  105.2 0.0 all-reduce.3.cloned.1.call-update
  105.2 53.4 %all-reduce.3.cloned.1.call-done = f32[8,4096]{1,0:T(8,128)} async-done(((f32[8,4096]{1,0:T(8,128)}), f32[8,4096]{1,0:T(8,128)}) %all-reduce.3.cloned.1.call-update) | async-done | bytes 131088 | tf_op jit(solution)/shard_map/psum | solution.py:101
  158.5 1.1 fusion.18
  159.6 0.7 add_convert_fusion
  (25 shorter events, 0.3 us)
Async XLA Ops:
  7.2 16.1 %copy-start = (bf16[4096,8,32]{0,2,1:T(8,128)(2,1)S(1)}, bf16[4096,8,32]{0,2,1:T(8,128)(2,1)}, u32[]{:S(2)}) copy-start(bf16[4096,8,32]{0,2,1:T(8,128)(2,1)} %param.17) | copy-start | bytes 6291460
  7.2 151.4 %all-reduce.3.cloned.1.call-start = ((), (), s32[]{:S(2)}) async-start(), calls=%async_computation.1 | async-start | bytes 262144 | tf_op jit(solution)/shard_map/psum | solution.py:101
  7.2 16.7 %copy-start.4 = (bf16[4096,8,32]{0,2,1:T(8,128)(2,1)S(1)}, bf16[4096,8,32]{0,2,1:T(8,128)(2,1)}, u32[]{:S(2)}) copy-start(bf16[4096,8,32]{0,2,1:T(8,128)(2,1)} %param.18) | copy-start | bytes 6291460
  23.9 3.2 %copy-start.2 = (bf16[4096,8,64]{0,2,1:T(8,128)(2,1)S(1)}, bf16[4096,8,64]{0,2,1:T(8,128)(2,1)}, u32[]{:S(2)}) copy-start(bf16[4096,8,64]{0,2,1:T(8,128)(2,1)} %param.19) | copy-start | bytes 12582916
  27.2 2.2 %copy-start.3 = (bf16[4096,8,64]{0,2,1:T(8,128)(2,1)S(1)}, bf16[4096,8,64]{0,2,1:T(8,128)(2,1)}, u32[]{:S(2)}) copy-start(bf16[4096,8,64]{0,2,1:T(8,128)(2,1)} %param.20) | copy-start | bytes 12582916
  29.4 12.1 %copy-start.7 = (f32[8,128]{1,0:T(8,128)S(1)}, f32[8,128]{1,0:T(8,128)}, u32[]{:S(2)}) copy-start(f32[8,128]{1,0:T(8,128)} %param.22) | copy-start | bytes 12292
  43.4 1.3 copy-start.1
  43.4 2.7 %copy-start.6 = (f32[8,256]{1,0:T(8,128)S(1)}, f32[8,256]{1,0:T(8,128)}, u32[]{:S(2)}) copy-start(f32[8,256]{1,0:T(8,128)} %param.24) | copy-start | bytes 24580
  43.4 16.9 %copy-start.5 = (bf16[8,512]{1,0:T(8,128)(2,1)S(1)}, bf16[8,512]{1,0:T(8,128)(2,1)}, u32[]{:S(2)}) copy-start(bf16[8,512]{1,0:T(8,128)(2,1)} %param.16) | copy-start | bytes 24580
  60.3 17.3 %copy-start.8 = (f32[512]{0:T(512)S(1)}, f32[512]{0:T(512)}, u32[]{:S(2)}) copy-start(f32[512]{0:T(512)} %param.27) | copy-start | bytes 6148
  60.3 17.3 %copy-start.9 = (f32[512]{0:T(512)S(1)}, f32[512]{0:T(512)}, u32[]{:S(2)}) copy-start(f32[512]{0:T(512)} %param.26) | copy-start | bytes 6148
  91.6 68.0 %copy-start.10 = (f32[512]{0:T(512)S(1)}, f32[512]{0:T(512)}, u32[]{:S(2)}) copy-start(f32[512]{0:T(512)} %param.31) | copy-start | bytes 6148
  91.6 68.0 %copy-start.11 = (f32[512]{0:T(512)S(1)}, f32[512]{0:T(512)}, u32[]{:S(2)}) copy-start(f32[512]{0:T(512)} %param.30) | copy-start | bytes 6148
Sparse Core Ops, SparseCore 0:
  105.3 53.1 all-reduce.2
where the time goes:
time: 167 us
  blocking collectives  68.3 us (41%)
  waiting for transfers between devices  53.4 us (32%)
  matrix products  23.9 us (14%)
  between operations  14.2 us (9%)
  other arithmetic  4 us (2%)
  local copies, waits for them, and re-layouts  3.36 us (2%)
    psum x1, waiting for transfers between devices, body(): mixer_all = lax.psum(mixer_term, ('kv', 'tp'))  53.4 us
    all_gather x1, blocking collectives, body(): whole = lax.all_gather(tokens, ('kv', 'tp'), axis=1, tiled=True)  16 us
    psum x1, blocking collectives, body(): lax.psum((jnp.sum(residual_one, axis=-1, keepdims=True), jnp.sum(residual...  14.2 us
    all_gather x1, blocking collectives, body(): lax.all_gather(attended.reshape(1, seq_count, flat_width), ('kv', 'tp'),...  14 us
    all_gather x1, blocking collectives, body(): normed = lax.all_gather(normed_own, ('kv', 'tp'), axis=1, tiled=True)  14 us
    dot_general x1, matrix products, body(): jnp.dot(hidden, down_weight, preferred_element_type=jnp.float32)  13.5 us
    all_to_all x1, blocking collectives, body(): lax.all_to_all(packed, 'kv', split_axis=0, concat_axis=0, tiled=True)  10.1 us
    dot_general x5, matrix products, project_flat(): jnp.dot(inputs, flattened, preferred_element_type=jnp.float32)  6.25 us
  transfers between devices with their start and end apart: 1, of which 1 were waited for; matrix products, arithmetic and copies ran while one was open for 0% of the time, Pallas kernels for 0%

commit v1 on v0

--- a/solution.py
+++ b/solution.py
@@ -98,7 +98,8 @@
     lifted = jnp.dot(normed, up_weight, preferred_element_type=jnp.float32)
     hidden = jnp.square(jax.nn.relu(lifted)).astype(jnp.bfloat16)
     mixer_term = jnp.dot(hidden, down_weight, preferred_element_type=jnp.float32)
-    mixer_all = lax.psum(mixer_term, ("kv", "tp"))
+    blocks = lax.all_gather(mixer_term, ("kv", "tp"), axis=0, tiled=False)
+    mixer_all = blocks.sum(axis=0)
     residual_two = ALPHA * normed.astype(jnp.float32) + mixer_all
     average = jnp.sum(residual_two, axis=-1, keepdims=True) / D
     spread = jnp.sum(residual_two * residual_two, axis=-1, keepdims=True) / D - average * average

time: 167 us -> 135 us (0.81)
  waiting for transfers between devices: 53.4 us -> 20.6 us
    psum x1 -> x0, waiting for transfers between devices: 53.4 us -> none  [body(): mixer_all = lax.psum(mixer_term, ('kv', 'tp'))]
    all_gather x0 -> x1, waiting for transfers between devices: none -> 20.6 us  [body(): blocks = lax.all_gather(mixer_term, ('kv', 'tp'), axis=0, tiled=False)]
where the time goes in v1:
time: 135 us
  blocking collectives  68.3 us (51%)
  matrix products  23.9 us (18%)
  waiting for transfers between devices  20.6 us (15%)
  between operations  14.2 us (11%)
  other arithmetic  4.38 us (3%)
  local copies, waits for them, and re-layouts  3.36 us (2%)
    all_gather x1, waiting for transfers between devices, body(): blocks = lax.all_gather(mixer_term, ('kv', 'tp'), axis=0, tiled=False)  20.6 us
    all_gather x1, blocking collectives, body(): whole = lax.all_gather(tokens, ('kv', 'tp'), axis=1, tiled=True)  16 us
    psum x1, blocking collectives, body(): lax.psum((jnp.sum(residual_one, axis=-1, keepdims=True), jnp.sum(residual...  14.2 us
    all_gather x1, blocking collectives, body(): lax.all_gather(attended.reshape(1, seq_count, flat_width), ('kv', 'tp'),...  14 us
    all_gather x1, blocking collectives, body(): normed = lax.all_gather(normed_own, ('kv', 'tp'), axis=1, tiled=True)  14 us
    dot_general x1, matrix products, body(): jnp.dot(hidden, down_weight, preferred_element_type=jnp.float32)  13.5 us
    all_to_all x1, blocking collectives, body(): lax.all_to_all(packed, 'kv', split_axis=0, concat_axis=0, tiled=True)  10.1 us
    dot_general x5, matrix products, project_flat(): jnp.dot(inputs, flattened, preferred_element_type=jnp.float32)  6.25 us
  transfers between devices with their start and end apart: 1, of which 1 were waited for; matrix products, arithmetic and copies ran while one was open for 0% of the time, Pallas kernels for 0%

profile of v1, /device:TPU:0, one launch (start us, length us, event | category | flops | bytes accessed | tf_op | source)
XLA Modules:
  0.0 134.8 jit_solution(10288028128793730151)
XLA Ops:
  7.2 0.0 copy-start
  7.2 0.0 all-gather.3.cloned.1.call-start
  7.2 0.0 copy-start.4
  7.2 16.0 %all_gather.15 = bf16[8,4096]{1,0:T(8,128)(2,1)S(1)} all-gather(bf16[8,512]{1,0:T(8,128)(2,1)} %param.16), channel_id=1, replica_groups=mesh['dp'=4,'kv'=4,'tp'=2] {'kv','tp'}, dimensions={1}, use_global_device_ids=true | all-gather | bytes 73728 | tf_op jit(solution)/shard_map/all_gather | solution.py:43
  23.3 0.0 copy-done
  23.3 0.6 fusion.7
  23.9 0.0 copy-done.4
  23.9 0.7 fusion.6
  24.6 2.6 %fusion.5 = bf16[8,1792]{1,0:T(8,128)(2,1)S(1)} fusion(bf16[8,1792]{1,0:T(8,128)(2,1)S(1)} %fusion.6, bf16[8,4096]{1,0:T(8,128)(2,1)S(1)} %all_gather.15, bf16[4096,256]{0,1:T(8,128)(2,1)} %bitcast.62), kind=kOutput, calls=%fused_computation.11 | convolution fusion | flops 16779264 | bytes 2166784 | tf_op jit(solution)/shard_map/dot_general | solution.py:16
  27.2 0.0 copy-done.2
  27.2 1.2 fusion.4
  28.4 1.0 copy-done.3
  29.4 1.2 fusion.3
  30.6 10.1 %all_to_all.12 = bf16[4,2,1792]{2,1,0:T(2,128)(2,1)S(1)} all-to-all(bf16[4,2,1792]{2,1,0:T(2,128)(2,1)S(1)} %all_to_all.8), channel_id=1, replica_groups=mesh['dp'=4,'kv'=4,'tp'=2] {'kv'}, dimensions={0} | all-to-all | bytes 57344 | tf_op jit(solution)/shard_map/all_to_all | solution.py:46
  40.7 0.1 reshape.138
  40.8 0.1 reshape.134
  40.9 0.1 reshape.136
  41.0 0.1 reshape.132
  41.1 0.1 reshape.137
  41.2 0.1 reshape.133
  41.3 0.1 mul.135
  41.4 0.1 reshape.141
  41.4 0.0 copy-done.7
  41.5 1.9 %multiply_add_fusion = f32[2,8,128,256]{3,2,1,0:T(8,128)S(1)} fusion(f32[2,8,128,256]{3,2,1,0:T(8,128)} %param.23, f32[2,8,256]{2,1,0:T(8,128)S(1)} %reshape.134, f32[2,8,128]{2,1,0:T(8,128)S(1)} %reshape.133, f32[2,8,128]{2,1,0:T(8,128)S(1)} %fusion.16), kind=kLoop, calls=%fused_computation.3 | loop fusion | flops 1572864 | bytes 4227072 | tf_op jit(solution)/shard_map/add | solution.py:65
  43.4 0.0 copy-start.1
  43.4 0.0 copy-start.6
  43.4 0.0 copy-start.5
  43.4 1.3 copy-done.1
  44.7 1.1 fusion.20
  45.8 0.1 fusion.10
  45.9 0.1 reshape.139
  46.0 0.1 reshape.135
  46.1 0.0 copy-done.6
  46.1 0.1 fusion.13
  46.2 14.0 %all_gather.16 = bf16[8,2,2048]{2,1,0:T(2,128)(2,1)S(1)} all-gather(bf16[1,2,2048]{2,1,0:T(2,128)(2,1)S(1)} %reshape.129), channel_id=1, replica_groups=mesh['dp'=4,'kv'=4,'tp'=2] {'kv','tp'}, dimensions={0}, use_global_device_ids=true | all-gather | bytes 73728 | tf_op jit(solution)/shard_map/all_gather | solution.py:75
  60.3 0.0 copy-start.8
  60.3 0.0 copy-start.9
  60.3 3.0 %fusion.19 = (f32[8]{0:T(128)S(1)}, f32[8]{0:T(128)S(1)}, f32[8,512]{1,0:T(8,128)S(1)}) fusion(bf16[8,2048,2]{1,0,2:T(8,128)(2,1)S(1)} %dot_general.38, bf16[2,2048,512]{2,1,0:T(8,128)(2,1)} %bitcast.58, bf16[8,512]{1,0:T(8,128)(2,1)S(1)} %copy-done.5), kind=kOutput, calls=%fused_computation.46 | convolution fusion | flops 33578992 | bytes 4284480 | tf_op jit(solution)/shard_map/atsc,tcd->asd/dot_general | solution.py:82
  63.3 14.2 %all-reduce = (f32[8,1]{0,1:T(1,128)S(1)}, f32[8,1]{0,1:T(1,128)S(1)}) all-reduce(f32[8,1]{0,1:T(1,128)S(1)} %bitcast.71, f32[8,1]{0,1:T(1,128)S(1)} %bitcast.70), channel_id=1, replica_groups=mesh['dp'=4,'kv'=4,'tp'=2] {'kv','tp'}, use_global_device_ids=true, to_apply=%region_4.5 | all-reduce | flops 16 | bytes 128 | tf_op jit(solution)/shard_map/psum | solution.py:87
  77.6 0.0 copy-done.9
  77.6 0.1 add_convert_fusion.1
  77.7 14.0 %all_gather.17 = bf16[8,4096]{1,0:T(8,128)(2,1)S(1)} all-gather(bf16[8,512]{1,0:T(8,128)(2,1)S(1)} %add_convert_fusion.1), channel_id=1, replica_groups=mesh['dp'=4,'kv'=4,'tp'=2] {'kv','tp'}, dimensions={1}, use_global_device_ids=true | all-gather | bytes 73728 | tf_op jit(solution)/shard_map/all_gather | solution.py:97
  91.6 13.5 %fusion.8 = f32[8,4096]{1,0:T(8,128)} fusion(bf16[2048,4096]{1,0:T(8,128)(2,1)} %param.29, bf16[8,4096]{1,0:T(8,128)(2,1)S(1)} %all_gather.17, bf16[4096,2048]{1,0:T(8,128)(2,1)} %param.28), kind=kOutput, calls=%fused_computation.17 | convolution fusion | flops 268484608 | bytes 33751040 | tf_op jit(solution)/shard_map/dot_general | solution.py:100
  105.2 0.0 all-gather.3.cloned.1.call-update
  105.2 20.6 %all-gather.3.cloned.1.call-done = f32[64,4096]{1,0:T(8,128)} async-done(((f32[8,4096]{1,0:T(8,128)}), f32[64,4096]{1,0:T(8,128)}) %all-gather.3.cloned.1.call-update) | async-done | bytes 1048592 | tf_op jit(solution)/shard_map/all_gather | solution.py:101
  125.8 1.3 bitcast_reduce_fusion
  127.1 0.2 fusion.18
  127.3 0.7 add_convert_fusion
  (26 shorter events, 0.3 us)
Async XLA Ops:
  7.2 16.1 %copy-start = (bf16[4096,8,32]{0,2,1:T(8,128)(2,1)S(1)}, bf16[4096,8,32]{0,2,1:T(8,128)(2,1)}, u32[]{:S(2)}) copy-start(bf16[4096,8,32]{0,2,1:T(8,128)(2,1)} %param.17) | copy-start | bytes 6291460
  7.2 118.6 %all-gather.3.cloned.1.call-start = ((), (), s32[]{:S(2)}) async-start(), calls=%async_computation.1 | async-start | bytes 1179648 | tf_op jit(solution)/shard_map/all_gather | solution.py:101
  7.2 16.7 %copy-start.4 = (bf16[4096,8,32]{0,2,1:T(8,128)(2,1)S(1)}, bf16[4096,8,32]{0,2,1:T(8,128)(2,1)}, u32[]{:S(2)}) copy-start(bf16[4096,8,32]{0,2,1:T(8,128)(2,1)} %param.18) | copy-start | bytes 6291460
  23.9 3.2 %copy-start.2 = (bf16[4096,8,64]{0,2,1:T(8,128)(2,1)S(1)}, bf16[4096,8,64]{0,2,1:T(8,128)(2,1)}, u32[]{:S(2)}) copy-start(bf16[4096,8,64]{0,2,1:T(8,128)(2,1)} %param.19) | copy-start | bytes 12582916
  27.2 2.2 %copy-start.3 = (bf16[4096,8,64]{0,2,1:T(8,128)(2,1)S(1)}, bf16[4096,8,64]{0,2,1:T(8,128)(2,1)}, u32[]{:S(2)}) copy-start(bf16[4096,8,64]{0,2,1:T(8,128)(2,1)} %param.20) | copy-start | bytes 12582916
  29.4 12.1 %copy-start.7 = (f32[8,128]{1,0:T(8,128)S(1)}, f32[8,128]{1,0:T(8,128)}, u32[]{:S(2)}) copy-start(f32[8,128]{1,0:T(8,128)} %param.22) | copy-start | bytes 12292
  43.4 1.3 copy-start.1
  43.4 2.7 %copy-start.6 = (f32[8,256]{1,0:T(8,128)S(1)}, f32[8,256]{1,0:T(8,128)}, u32[]{:S(2)}) copy-start(f32[8,256]{1,0:T(8,128)} %param.24) | copy-start | bytes 24580
  43.4 16.9 %copy-start.5 = (bf16[8,512]{1,0:T(8,128)(2,1)S(1)}, bf16[8,512]{1,0:T(8,128)(2,1)}, u32[]{:S(2)}) copy-start(bf16[8,512]{1,0:T(8,128)(2,1)} %param.16) | copy-start | bytes 24580
  60.3 17.3 %copy-start.8 = (f32[512]{0:T(512)S(1)}, f32[512]{0:T(512)}, u32[]{:S(2)}) copy-start(f32[512]{0:T(512)} %param.27) | copy-start | bytes 6148
  60.3 17.3 %copy-start.9 = (f32[512]{0:T(512)S(1)}, f32[512]{0:T(512)}, u32[]{:S(2)}) copy-start(f32[512]{0:T(512)} %param.26) | copy-start | bytes 6148
  91.6 35.6 %copy-start.10 = (f32[512]{0:T(512)S(1)}, f32[512]{0:T(512)}, u32[]{:S(2)}) copy-start(f32[512]{0:T(512)} %param.31) | copy-start | bytes 6148
  91.6 35.6 %copy-start.11 = (f32[512]{0:T(512)S(1)}, f32[512]{0:T(512)}, u32[]{:S(2)}) copy-start(f32[512]{0:T(512)} %param.30) | copy-start | bytes 6148
Sparse Core Ops, SparseCore 0:
  105.3 20.4 all-gather.2
